TPU v7x, 32 devices: a whole 2x2x4 slice. The times are simulated.
32 devices in a mesh: fs: 4 (over z), tp: 8 (over y, x, core).
Axes of the slice: x: 2, y: 2, z: 4, core: 2. Of those that a mesh axis runs over, the one named last changes fastest.
Arguments:
- tokens: bfloat16 [768, 2304], P('fs'), may hold values from -6 to 6
- gate_train: float32 [8, 2304, 2304], P(None, 'fs', 'tp'), may hold values from -0.125 to 0.125
- up_train: float32 [8, 2304, 2304], P(None, 'fs', 'tp'), may hold values from -0.125 to 0.125
- down_train: float32 [8, 2304, 2304], P(None, 'fs', 'tp'), may hold values from -0.125 to 0.125
- gain: float32 [2304], P('fs'), may hold values from 0.1 to 1.9
- routes: int32 [768, 2], P('fs'), may hold values from 0 to 7, all different within a row; in each aligned block of 192 rows (0 to 191, 192 to 383, ...) at most 72 rows name the same one
- route_weights: float32 [768, 2], P('fs'), may hold values from 0.1 to 1
Outputs:
- gate_new: bfloat16 [8, 2304, 2304], P('tp')
- up_new: bfloat16 [8, 2304, 2304], P('tp')
- down_new: bfloat16 [8, 2304, 2304], P('tp')
- mixed: bfloat16 [768, 2304], P('fs', 'tp')
Inputs may be any that keep to these rules, and one draw needn't show every extreme that they name: `routes`: each row names two different experts; in each aligned block of 192 rows at most 72 rows name one expert, a bound that some block reaches.
All inputs are finite; a program needn't handle non-finite values.
Results may differ from a plain program's by a relative error of at most 0.0095.
Values may be sent and summed in bfloat16 or wider, within the bound.
A program may use at most 128 MiB of HBM per device.

v0:
```python
import jax
import jax.numpy as jnp
from jax import lax
from jax.sharding import PartitionSpec as P

CAP = 72


norm_eps = 1e-06


def arrange(matrix, tp_count):
    experts, row_count, col_count = matrix.shape
    slices = tp_count // experts
    piece_width = col_count // slices
    shaped = matrix.reshape(experts, row_count, slices, piece_width)
    return shaped.transpose(0, 2, 3, 1).reshape(tp_count, piece_width, row_count)


def shards(tokens, gate_train, up_train, down_train, gain, routes, route_weights):
    tp_count = lax.axis_size("tp")
    experts = gate_train.shape[0]
    slices = tp_count // experts
    gain_column = gain[None, :, None]
    gate_round = (gate_train * gain_column).astype(jnp.bfloat16)
    up_round = (up_train * gain_column).astype(jnp.bfloat16)
    down_round = down_train.astype(jnp.bfloat16)
    moved = (
        lax.all_to_all(
            arrange(gate_round, tp_count), "tp", split_axis=0, concat_axis=1, tiled=True
        ),
        lax.all_to_all(arrange(up_round, tp_count), "tp", split_axis=0, concat_axis=1, tiled=True),
        lax.all_to_all(
            arrange(down_round, tp_count), "tp", split_axis=0, concat_axis=1, tiled=True
        ),
    )
    tokens_wide = tokens.astype(jnp.float32)
    normed = (
        tokens_wide
        * lax.rsqrt(jnp.mean(tokens_wide * tokens_wide, axis=1, keepdims=True) + norm_eps)
    ).astype(jnp.bfloat16)
    expert = lax.axis_index("tp") // slices
    matches = routes == expert
    member = jnp.any(matches, axis=1)
    slot_index = jnp.cumsum(member.astype(jnp.int32)) - 1
    marked = jnp.where(member, slot_index, -1)
    picker = (marked[None, :] == jnp.arange(CAP, dtype=jnp.int32)[:, None]).astype(jnp.bfloat16)
    chosen = jnp.dot(picker, normed, preferred_element_type=jnp.float32).astype(jnp.bfloat16)
    contract_last = (((1,), (1,)), ((), ()))
    gate_new, up_new, down_new = (
        lax.all_gather(moved[0], "fs", axis=2, tiled=True),
        lax.all_gather(moved[1], "fs", axis=2, tiled=True),
        lax.all_gather(moved[2], "fs", axis=2, tiled=True),
    )
    gate_pre = lax.dot_general(
        chosen, gate_new[0], contract_last, preferred_element_type=jnp.float32
    )
    up_pre = lax.dot_general(chosen, up_new[0], contract_last, preferred_element_type=jnp.float32)
    hidden = (jax.nn.silu(gate_pre) * up_pre).astype(jnp.bfloat16)
    partial_value = jnp.dot(hidden, down_new[0], preferred_element_type=jnp.float32).astype(
        jnp.bfloat16
    )
    labels = jnp.arange(experts, dtype=jnp.int32)
    member_all = jnp.any(routes[:, :, None] == labels[None, None, :], axis=1)
    slots_all = jnp.cumsum(member_all.astype(jnp.int32), axis=0) - 1
    slot_pair = jnp.take_along_axis(slots_all, routes, axis=1)
    flat_index = slot_pair * experts + routes
    received = lax.all_to_all(
        partial_value.reshape(CAP, tp_count, -1), "tp", split_axis=1, concat_axis=1, tiled=True
    )
    summed = jnp.sum(received.reshape(CAP, experts, slices, -1).astype(jnp.float32), axis=2)
    summed = summed.reshape(CAP * experts, -1)
    picked = jnp.take(summed, flat_index, axis=0)
    mixed = jnp.sum(route_weights[:, :, None] * picked, axis=1)
    return (gate_new, up_new, down_new, mixed.astype(jnp.bfloat16))


def solution(mesh):
    in_specs = (
        P("fs", None),
        P(None, "fs", "tp"),
        P(None, "fs", "tp"),
        P(None, "fs", "tp"),
        P("fs"),
        P("fs", None),
        P("fs", None),
    )
    out_specs = (P("tp", None, None), P("tp", None, None), P("tp", None, None), P("fs", "tp"))
    return jax.shard_map(shards, mesh=mesh, in_specs=in_specs, out_specs=out_specs, check_vma=False)
```

profile of v0, /device:TPU:0, one launch (start us, length us, event | category | flops | bytes accessed | tf_op | source)
XLA Modules:
  0.0 690.3 jit_solution(4470130244694976679)
XLA Ops:
  7.2 5.4 fusion.16
  12.6 40.8 %all_to_all.41 = bf16[8,288,576]{2,1,0:T(8,128)(2,1)} all-to-all(bf16[8,288,576]{2,1,0:T(8,128)(2,1)S(1)} %get-tuple-element.23), channel_id=1, replica_groups=mesh['fs'=4,'tp'=8] {'tp'}, dimensions={0} | all-to-all | bytes 5308416 | tf_op jit(solution)/shard_map/all_to_all | solution.py:29
  53.4 4.5 copy.89
  57.9 38.9 %all_to_all.42 = bf16[8,288,576]{2,1,0:T(8,128)(2,1)} all-to-all(bf16[8,288,576]{2,1,0:T(8,128)(2,1)S(1)} %get-tuple-element.22), channel_id=1, replica_groups=mesh['fs'=4,'tp'=8] {'tp'}, dimensions={0} | all-to-all | bytes 5308416 | tf_op jit(solution)/shard_map/all_to_all | solution.py:32
  96.9 4.5 copy.90
  101.4 3.0 convert_bitcast_fusion
  104.5 38.1 %all_to_all.43 = bf16[8,288,576]{2,1,0:T(8,128)(2,1)S(1)} all-to-all(bf16[8,288,576]{2,1,0:T(8,128)(2,1)S(1)} %convert_bitcast_fusion), channel_id=1, replica_groups=mesh['fs'=4,'tp'=8] {'tp'}, dimensions={0} | all-to-all | bytes 5308416 | tf_op jit(solution)/shard_map/all_to_all | solution.py:33
  142.6 3.4 copy.91
  146.0 0.6 reduce-window.15
  146.6 0.2 slice_reduce_fusion
  147.0 0.1 reshape.127
  147.3 2.7 gather_fusion.1
  149.9 0.1 reshape.130
  150.2 0.3 reduce-window.19
  150.8 0.3 fusion.17
  151.1 0.4 convolution_convert_fusion
  151.5 92.0 %all-gather.4.cloned.1.call-done = bf16[1,2304,2304]{1,2,0:T(8,128)(2,1)} async-done(((bf16[1,2304,576]{1,2,0:T(8,128)(2,1)}), bf16[1,2304,2304]{1,2,0:T(8,128)(2,1)}) %all-gather.4.cloned.1.call-update) | async-done | bytes 10616848 | tf_op jit(solution)/shard_map/all_gather | solution.py:51
  243.4 6.0 fusion.4
  249.4 180.4 %all-gather.6.cloned.1.call-done = bf16[1,2304,2304]{1,2,0:T(8,128)(2,1)} async-done(((bf16[1,2304,576]{1,2,0:T(8,128)(2,1)}), bf16[1,2304,2304]{1,2,0:T(8,128)(2,1)}) %all-gather.6.cloned.1.call-update) | async-done | bytes 10616848 | tf_op jit(solution)/shard_map/all_gather | solution.py:52
  429.8 186.4 %all-gather.8.cloned.1.call-done = bf16[1,2304,2304]{1,2,0:T(8,128)(2,1)} async-done(((bf16[1,2304,576]{1,2,0:T(8,128)(2,1)}), bf16[1,2304,2304]{1,2,0:T(8,128)(2,1)}) %all-gather.8.cloned.1.call-update) | async-done | bytes 10616848 | tf_op jit(solution)/shard_map/all_gather | solution.py:53
  616.2 11.9 %fusion.12 = bf16[72,2304]{1,0:T(8,128)(2,1)S(1)} fusion(bf16[1,2304,2304]{1,2,0:T(8,128)(2,1)} %all-gather.8.cloned.1.call-done, bf16[72,2304]{1,0:T(8,128)(2,1)S(1)} %convolution_convert_fusion, bf16[1,2304,2304]{1,2,0:T(8,128)(2,1)} %all-gather.6.cloned.1.call-done, f32[72,2304]{1,0:T(8,128)S(1)} %fusion.4), kind=kOutput, calls=%fused_computation.12 | convolution fusion | flops 1529985024 | bytes 22560768 | tf_op jit(solution)/shard_map/dot_general | solution.py:60
  628.2 0.7 reshape.112
  628.8 0.8 copy.96
  629.7 3.7 all-to-all-start.3
  633.5 0.1 reshape.121
  633.6 0.2 copy.95
  633.9 15.2 %copy.100 = bf16[1,2304,2304]{2,1,0:T(8,128)(2,1)} copy(bf16[1,2304,2304]{1,2,0:T(8,128)(2,1)} %all-gather.6.cloned.1.call-done) | data formatting | bytes 21233664
  649.1 15.2 %copy.99 = bf16[1,2304,2304]{2,1,0:T(8,128)(2,1)} copy(bf16[1,2304,2304]{1,2,0:T(8,128)(2,1)} %all-gather.4.cloned.1.call-done) | data formatting | bytes 21233664
  664.3 15.2 %copy.101 = bf16[1,2304,2304]{2,1,0:T(8,128)(2,1)} copy(bf16[1,2304,2304]{1,2,0:T(8,128)(2,1)} %all-gather.8.cloned.1.call-done) | data formatting | bytes 21233664
  679.6 1.7 gather_fusion
  681.4 0.3 reshape.120
  681.7 2.0 multiply_reduce_fusion
  (34 shorter events, 1.2 us)
Async XLA Ops:
  7.2 236.3 %all-gather.4.cloned.1.call-start = ((), (), s32[]{:S(2)}) async-start(), calls=%async_computation.4 | async-start | bytes 13271040 | tf_op jit(solution)/shard_map/all_gather | solution.py:51
  57.9 372.0 %all-gather.6.cloned.1.call-start = ((), (), s32[]{:S(2)}) async-start(), calls=%async_computation.5 | async-start | bytes 13271040 | tf_op jit(solution)/shard_map/all_gather | solution.py:52
  101.4 514.9 %all-gather.8.cloned.1.call-start = ((), (), s32[]{:S(2)}) async-start(), calls=%async_computation.6 | async-start | bytes 13271040 | tf_op jit(solution)/shard_map/all_gather | solution.py:53
  104.5 41.6 %copy-start.1 = (s32[192,2]{0,1:T(2,128)S(1)}, s32[192,2]{0,1:T(2,128)}, u32[]{:S(2)}) copy-start(s32[192,2]{0,1:T(2,128)} %param.12) | copy-start | bytes 4612
  147.3 3.5 copy-start
  249.4 384.3 %copy-start.2 = (f32[192,2]{0,1:T(2,128)S(1)}, f32[192,2]{0,1:T(2,128)}, u32[]{:S(2)}) copy-start(f32[192,2]{0,1:T(2,128)} %param.13) | copy-start | bytes 4612
  629.7 49.9 %all-to-all-start.3 = ((bf16[72,8,288]{2,0,1:T(8,128)(2,1)}), bf16[72,8,288]{2,0,1:T(8,128)(2,1)S(1)}, u32[]{:S(2)}, u32[]{:S(2)}) async-start(bf16[72,8,288]{2,0,1:T(8,128)(2,1)} %copy.96), calls=%async_computation.3 | async-start | bytes 884736 | tf_op jit(solution)/shard_map/all_to_all | solution.py:68
Sparse Core Ops, SparseCore 0:
  58.0 185.3 all-gather.3
  245.6 184.2 all-gather.5
  432.0 184.2 all-gather.7
where the time goes:
time: 692 us; the launch traced here: 690 us
  waiting for transfers between devices  459 us (66%)
  blocking collectives  118 us (17%)
  local copies, waits for them, and re-layouts  65.7 us (9%)
  matrix products  18.3 us (3%)
  between operations  13.9 us (2%)
  other arithmetic  11.9 us (2%)
    all_gather x1, waiting for transfers between devices, shards(): lax.all_gather(moved[2], 'fs', axis=2, tiled=True)  186 us
    all_gather x1, waiting for transfers between devices, shards(): lax.all_gather(moved[1], 'fs', axis=2, tiled=True)  180 us
    all_gather x1, waiting for transfers between devices, shards(): lax.all_gather(moved[0], 'fs', axis=2, tiled=True)  92 us
    unnamed x10, local copies, waits for them, and re-layouts  45.8 us
    all_to_all x1, blocking collectives, shards(): lax.all_to_all(arrange(gate_round, tp_count), 'tp', split_axis=0, concat_...  40.8 us
    all_to_all x1, blocking collectives, shards(): lax.all_to_all(arrange(up_round, tp_count), 'tp', split_axis=0, concat_ax...  38.9 us
    all_to_all x1, blocking collectives, shards(): lax.all_to_all(arrange(down_round, tp_count), 'tp', split_axis=0, concat_...  38.1 us
  transfers between devices with their start and end apart: 4, of which 3 were waited for; matrix products, arithmetic and copies ran while one was open for 10% of the time, Pallas kernels for 0%

commit v1 on v0

v1 whole, which is shorter than its diff:
```python
import jax
import jax.numpy as jnp
from jax import lax
from jax.experimental import pallas as pl
from jax.experimental.pallas import tpu as pltpu
from jax.sharding import PartitionSpec as P

CAP = 72


norm_eps = 1e-06


def arrange(matrix, tp_count):
    experts, row_count, col_count = matrix.shape
    slices = tp_count // experts
    piece_width = col_count // slices
    shaped = matrix.reshape(experts, row_count, slices, piece_width)
    return shaped.transpose(0, 2, 3, 1).reshape(tp_count, piece_width, row_count)


def block_of(*counts):
    for size in (256, 128):
        if all(count % size == 0 for count in counts):
            return size
    return None


def flip(wide, total_rows, first_row, base=None):
    features, rows = wide.shape
    size = block_of(rows, first_row, total_rows) or rows
    first = first_row // size

    def kernel(*refs):
        refs[-1][...] = refs[0][...].T

    in_specs = [pl.BlockSpec((features, size), lambda i: (0, i))]
    operands = [wide]
    aliases = {}
    if base is not None:
        in_specs.append(pl.BlockSpec(memory_space=pl.ANY))
        operands.append(base)
        aliases = {1: 0}
    return pl.pallas_call(
        kernel,
        grid=(rows // size,),
        in_specs=in_specs,
        out_specs=pl.BlockSpec((size, features), lambda i: (first + i, 0)),
        out_shape=jax.ShapeDtypeStruct((total_rows, features), wide.dtype),
        input_output_aliases=aliases,
        cost_estimate=pl.CostEstimate(
            flops=0, bytes_accessed=4 * features * rows, transcendentals=0
        ),
    )(*operands)


def flip_dot(wide, total_rows, hidden):
    features, rows = wide.shape
    size = block_of(rows, total_rows) or rows
    slots = hidden.shape[0]

    def kernel(wide_ref, hidden_ref, rows_ref, total_ref):
        turned = wide_ref[...].T
        rows_ref[...] = turned

        @pl.when(pl.program_id(0) == 0)
        def _():
            total_ref[...] = jnp.zeros_like(total_ref)

        total_ref[...] += jnp.dot(hidden_ref[...], turned, preferred_element_type=jnp.float32)

    return pl.pallas_call(
        kernel,
        grid=(rows // size,),
        in_specs=[
            pl.BlockSpec((features, size), lambda i: (0, i)),
            pl.BlockSpec((slots, size), lambda i: (0, i)),
        ],
        out_specs=[
            pl.BlockSpec((size, features), lambda i: (i, 0)),
            pl.BlockSpec((slots, features), lambda i: (0, 0)),
        ],
        out_shape=[
            jax.ShapeDtypeStruct((total_rows, features), wide.dtype),
            jax.ShapeDtypeStruct((slots, features), jnp.float32),
        ],
        cost_estimate=pl.CostEstimate(
            flops=2 * slots * features * rows,
            bytes_accessed=4 * features * rows,
            transcendentals=0,
        ),
    )(wide, hidden)


def keep_dot(weights, chosen):
    rows, features = weights.shape
    size = block_of(rows) or rows
    slots = chosen.shape[0]

    def kernel(weights_ref, chosen_ref, rows_ref, product_ref):
        rows_ref[...] = weights_ref[...]
        product_ref[...] = lax.dot_general(
            chosen_ref[...],
            weights_ref[...],
            (((1,), (1,)), ((), ())),
            preferred_element_type=jnp.float32,
        )

    return pl.pallas_call(
        kernel,
        grid=(rows // size,),
        in_specs=[
            pl.BlockSpec((size, features), lambda i: (i, 0)),
            pl.BlockSpec((slots, features), lambda i: (0, 0)),
        ],
        out_specs=[
            pl.BlockSpec((size, features), lambda i: (i, 0)),
            pl.BlockSpec((slots, size), lambda i: (0, i)),
        ],
        out_shape=[
            jax.ShapeDtypeStruct((rows, features), weights.dtype),
            jax.ShapeDtypeStruct((slots, rows), jnp.float32),
        ],
        cost_estimate=pl.CostEstimate(
            flops=2 * slots * features * rows,
            bytes_accessed=4 * features * rows,
            transcendentals=0,
        ),
    )(weights, chosen)


def after(value, *others):
    def kernel(*refs):
        pass

    return pl.pallas_call(
        kernel,
        in_specs=[pl.BlockSpec(memory_space=pl.ANY)] * (1 + len(others)),
        out_specs=pl.BlockSpec(memory_space=pl.ANY),
        out_shape=jax.ShapeDtypeStruct(value.shape, value.dtype),
        input_output_aliases={0: 0},
    )(value, *others)


def shards(tokens, gate_train, up_train, down_train, gain, routes, route_weights):
    tp_count = lax.axis_size("tp")
    experts = gate_train.shape[0]
    slices = tp_count // experts
    gain_column = gain[None, :, None]
    gate_round = (gate_train * gain_column).astype(jnp.bfloat16)
    up_round = (up_train * gain_column).astype(jnp.bfloat16)
    down_round = down_train.astype(jnp.bfloat16)

    def exchange(matrix):
        return lax.all_to_all(matrix, "tp", split_axis=0, concat_axis=1, tiled=True)

    local_features = gate_train.shape[1]
    gate_local = arrange(gate_round, tp_count).transpose(2, 0, 1).reshape(local_features, -1)
    gate_all = lax.all_gather(gate_local, "fs", axis=0, tiled=True)
    features = gate_all.shape[0]

    up_moved = exchange(arrange(up_round, tp_count))[0].T
    down_moved = exchange(arrange(down_round, tp_count))[0].T
    up_wide = lax.all_gather(up_moved, "fs", axis=0, tiled=True)

    units = down_moved.shape[1]
    size = block_of(units) or units
    main = units - size if units > size else units
    down_wide = lax.all_gather(down_moved[:, :main], "fs", axis=0, tiled=True)

    tokens_wide = tokens.astype(jnp.float32)
    normed = (
        tokens_wide
        * lax.rsqrt(jnp.mean(tokens_wide * tokens_wide, axis=1, keepdims=True) + norm_eps)
    ).astype(jnp.bfloat16)
    expert = lax.axis_index("tp") // slices
    matches = routes == expert
    member = jnp.any(matches, axis=1)
    slot_index = jnp.cumsum(member.astype(jnp.int32)) - 1
    marked = jnp.where(member, slot_index, -1)
    picker = (marked[None, :] == jnp.arange(CAP, dtype=jnp.int32)[:, None]).astype(jnp.bfloat16)
    chosen = jnp.dot(picker, normed, preferred_element_type=jnp.float32).astype(jnp.bfloat16)
    contract_last = (((1,), (1,)), ((), ()))

    gate_moved = exchange(gate_all.reshape(features, tp_count, -1).transpose(1, 2, 0))
    gate_new, gate_pre = keep_dot(gate_moved[0], chosen)
    up_new = flip(up_wide, units, 0)
    up_pre = jnp.dot(chosen, up_wide, preferred_element_type=jnp.float32)
    hidden = (jax.nn.silu(gate_pre) * up_pre).astype(jnp.bfloat16)
    down_new, partial_value = flip_dot(down_wide, units, hidden[:, :main])
    if main < units:
        rest_moved = after(down_moved[:, main:], up_new, gate_new, hidden)
        rest_wide = lax.all_gather(rest_moved, "fs", axis=0, tiled=True)
        partial_value = partial_value + lax.dot_general(
            hidden[:, main:], rest_wide, contract_last, preferred_element_type=jnp.float32
        )
        down_new = flip(rest_wide, units, main, down_new)
    partial_value = partial_value.astype(jnp.bfloat16)

    labels = jnp.arange(experts, dtype=jnp.int32)
    member_all = jnp.any(routes[:, :, None] == labels[None, None, :], axis=1)
    slots_all = jnp.cumsum(member_all.astype(jnp.int32), axis=0) - 1
    slot_pair = jnp.take_along_axis(slots_all, routes, axis=1)
    flat_index = slot_pair * experts + routes
    received = lax.all_to_all(
        partial_value.reshape(CAP, tp_count, -1), "tp", split_axis=1, concat_axis=1, tiled=True
    )
    summed = jnp.sum(received.reshape(CAP, experts, slices, -1).astype(jnp.float32), axis=2)
    summed = summed.reshape(CAP * experts, -1)
    picked = jnp.take(summed, flat_index, axis=0)
    mixed = jnp.sum(route_weights[:, :, None] * picked, axis=1)
    return (gate_new[None], up_new[None], down_new[None], mixed.astype(jnp.bfloat16))


def solution(mesh):
    in_specs = (
        P("fs", None),
        P(None, "fs", "tp"),
        P(None, "fs", "tp"),
        P(None, "fs", "tp"),
        P("fs"),
        P("fs", None),
        P("fs", None),
    )
    out_specs = (P("tp", None, None), P("tp", None, None), P("tp", None, None), P("fs", "tp"))
    return jax.shard_map(shards, mesh=mesh, in_specs=in_specs, out_specs=out_specs, check_vma=False)
```

time: 692 us -> 619 us (0.89)
  waiting for transfers between devices: 459 us -> 410 us
  Pallas kernels: 0 us -> 39.4 us
  blocking collectives: 118 us -> 78.9 us
  local copies, waits for them, and re-layouts: 65.7 us -> 42.4 us
  matrix products: 18.3 us -> 9.96 us
    all_gather x3 -> x4, waiting for transfers between devices: 459 us -> 404 us  [the longest x1 158 us: shards(): up_wide = lax.all_gather(up_moved, 'fs', axis=0, tiled=True)]
    unnamed x10 -> x11, local copies, waits for them, and re-layouts: 45.8 us -> 1.08 us
    pallas_call x0 -> x5, Pallas kernels: none -> 39.4 us  [the longest x2 15.5 us: flip(): pl.pallas_call(kernel, grid=(rows // size,), in_specs=in_specs, out_specs...]
    all_to_all x3 -> x2, blocking collectives: 118 us -> 78.9 us  [exchange(): return lax.all_to_all(matrix, 'tp', split_axis=0, concat_axis=1, tiled=True)]
    all_gather x0 -> x1, local copies, waits for them, and re-layouts: none -> 15.4 us  [shards(): gate_all = lax.all_gather(gate_local, 'fs', axis=0, tiled=True)]
    all_to_all x3 -> x0, local copies, waits for them, and re-layouts: 12.3 us -> none  [the longest x1 4.48 us: shards(): lax.all_to_all(arrange(gate_round, tp_count), 'tp', split_axis=0, concat_...]
    dot_general x2, matrix products: 17.9 us -> 8.85 us  [the longest x1 6.9 us: shards(): up_pre = jnp.dot(chosen, up_wide, preferred_element_type=jnp.float32)]
    squeeze x0 -> x2, local copies, waits for them, and re-layouts: none -> 7.98 us  [the longest x1 4.49 us: shards(): up_moved = exchange(arrange(up_round, tp_count))[0].T]
  transfers between devices with their start and end apart: 4 -> 6, of which waited for: 3 -> 5; matrix products, arithmetic and copies ran while one was open for 10% -> 7% of each run, Pallas kernels for 0% -> 6%
where the time goes in v1:
time: 619 us; the launch traced here: 617 us
  waiting for transfers between devices  410 us (66%)
  blocking collectives  78.9 us (13%)
  local copies, waits for them, and re-layouts  42.4 us (7%)
  Pallas kernels  39.4 us (6%)
  between operations  13.9 us (2%)
  other arithmetic  13.5 us (2%)
  matrix products  9.96 us (2%)
  starting transfers between devices  9.12 us (1%)
    all_gather x1, waiting for transfers between devices, shards(): up_wide = lax.all_gather(up_moved, 'fs', axis=0, tiled=True)  158 us
    all_gather x1, waiting for transfers between devices, shards(): down_wide = lax.all_gather(down_moved[:, :main], 'fs', axis=0, tiled=True)  131 us
    all_gather x1, waiting for transfers between devices, shards(): gate_all = lax.all_gather(gate_local, 'fs', axis=0, tiled=True)  95.5 us
    all_to_all x2, blocking collectives, exchange(): return lax.all_to_all(matrix, 'tp', split_axis=0, concat_axis=1, tiled=True)  78.9 us
    all_gather x1, waiting for transfers between devices, shards(): rest_wide = lax.all_gather(rest_moved, 'fs', axis=0, tiled=True)  19.6 us
    pallas_call x2, Pallas kernels, flip(): pl.pallas_call(kernel, grid=(rows // size,), in_specs=in_specs, out_specs...  15.5 us
    all_gather x1, local copies, waits for them, and re-layouts, shards(): gate_all = lax.all_gather(gate_local, 'fs', axis=0, tiled=True)  15.4 us
    pallas_call x1, Pallas kernels, keep_dot(): pl.pallas_call(kernel, grid=(rows // size,), in_specs=[pl.BlockSpec((size...  13.6 us
  transfers between devices with their start and end apart: 6, of which 5 were waited for; matrix products, arithmetic and copies ran while one was open for 7% of the time, Pallas kernels for 6%

profile of v1, /device:TPU:0, one launch (start us, length us, event | category | flops | bytes accessed | tf_op | source)
XLA Modules:
  0.0 617.1 jit_solution(13989617130235801951)
XLA Ops:
  7.2 7.0 %fusion.2 = (bf16[8,288,576]{2,1,0:T(8,128)(2,1)S(1)}, bf16[8,576,288]{1,2,0:T(8,128)(2,1)}) fusion(f32[8,576,288]{1,2,0:T(8,128)} %param.9, f32[576]{0:T(1024)} %param.11, f32[8,576,288]{1,2,0:T(8,128)} %param.8), kind=kLoop, calls=%fused_computation.9 | loop fusion | flops 5308416 | bytes 15927552 | tf_op jit(solution)/shard_map/reshape | solution.py:19
  14.2 4.5 copy.89
  18.7 40.8 %all_to_all.32 = bf16[8,288,576]{2,1,0:T(8,128)(2,1)} all-to-all(bf16[8,288,576]{2,1,0:T(8,128)(2,1)S(1)} %get-tuple-element.14), channel_id=1, replica_groups=mesh['fs'=4,'tp'=8] {'tp'}, dimensions={0} | all-to-all | bytes 5308416 | tf_op jit(solution)/shard_map/all_to_all | solution.py:155
  59.5 4.5 copy.91
  64.1 3.0 convert_bitcast_fusion
  67.1 38.1 %all_to_all.33 = bf16[8,288,576]{2,1,0:T(8,128)(2,1)S(1)} all-to-all(bf16[8,288,576]{2,1,0:T(8,128)(2,1)S(1)} %convert_bitcast_fusion), channel_id=1, replica_groups=mesh['fs'=4,'tp'=8] {'tp'}, dimensions={0} | all-to-all | bytes 5308416 | tf_op jit(solution)/shard_map/all_to_all | solution.py:155
  105.2 3.5 copy.92
  108.7 3.4 slice.46
  112.1 95.5 %all-gather.5.cloned.1.call-done = bf16[2304,2304]{1,0:T(8,128)(2,1)} async-done(((bf16[576,2304]{1,0:T(8,128)(2,1)}), bf16[2304,2304]{1,0:T(8,128)(2,1)}) %all-gather.5.cloned.1.call-update) | async-done | bytes 10616848 | tf_op jit(solution)/shard_map/all_gather | solution.py:159
  207.6 15.4 %copy.90 = bf16[2304,2304]{0,1:T(8,128)(2,1)} copy(bf16[2304,2304]{1,0:T(8,128)(2,1)} %all-gather.5.cloned.1.call-done) | data formatting | bytes 21233664 | tf_op jit(solution)/shard_map/all_gather | solution.py:159
  223.0 5.3 all-to-all-start
  228.4 0.6 reduce-window.19
  229.7 2.7 gather_fusion.1
  233.5 1.1 convolution_convert_fusion.chosen_ref
  234.6 1.7 slice.45.refs_0_
  236.3 157.7 %all-gather.7.cloned.1.call-done.refs_0_ = bf16[2304,2304]{1,0:T(8,128)(2,1)} async-done(((bf16[576,2304]{1,0:T(8,128)(2,1)}), bf16[2304,2304]{1,0:T(8,128)(2,1)}) %all-gather.7.cloned.1.call-update) | async-done | bytes 10616848 | tf_op jit(solution)/shard_map/all_gather | solution.py:164
  394.0 12.9 %shard_map.103.refs_1_ = bf16[2304,2304]{1,0:T(8,128)(2,1)} custom-call(bf16[2304,2304]{1,0:T(8,128)(2,1)} %all-gather.7.cloned.1.call-done.refs_0_), custom_call_target="tpu_custom_call" | custom-call | bytes 21233664 | tf_op jit(solution)/shard_map/pallas_call | solution.py:44
  406.9 13.6 %shard_map.102 = (bf16[2304,2304]{1,0:T(8,128)(2,1)}, f32[72,2304]{1,0:T(8,128)}) custom-call(bf16[2304,2304]{1,0:T(8,128)(2,1)} %bitcast.7.weights_ref, bf16[72,2304]{1,0:T(8,128)(2,1)} %convolution_convert_fusion.chosen_ref), custom_call_target="tpu_custom_call" | custom-call | flops 764411904 | bytes 21233664 | tf_op jit(solution)/shard_map/pallas_call | solution.py:109
  420.5 6.9 %fusion.refs_3_ = bf16[72,2304]{1,0:T(8,128)(2,1)} fusion(bf16[72,2304]{1,0:T(8,128)(2,1)S(1)} %copy-done, bf16[2304,2304]{1,0:T(8,128)(2,1)} %all-gather.7.cloned.1.call-done.refs_0_, f32[72,2304]{1,0:T(8,128)} %get-tuple-element.9), kind=kOutput, calls=%fused_computation.6 | convolution fusion | flops 765407232 | bytes 11943936 | tf_op jit(solution)/shard_map/dot_general | solution.py:188
  427.4 1.0 copy-done.2
  428.4 0.7 slice.47.hidden_ref
  429.1 131.4 %all-gather.11.cloned.1.call-done.wide_ref = bf16[2304,2048]{1,0:T(8,128)(2,1)} async-done(((bf16[576,2048]{1,0:T(8,128)(2,1)}), bf16[2304,2048]{1,0:T(8,128)(2,1)}) %all-gather.11.cloned.1.call-update) | async-done | bytes 9437200 | tf_op jit(solution)/shard_map/all_gather | solution.py:169
  560.5 10.3 %shard_map.105 = (bf16[2304,2304]{1,0:T(8,128)(2,1)}, f32[72,2304]{1,0:T(8,128)}) custom-call(bf16[2304,2048]{1,0:T(8,128)(2,1)} %all-gather.11.cloned.1.call-done.wide_ref, bf16[72,2048]{1,0:T(8,128)(2,1)} %slice.47.hidden_ref), custom_call_target="tpu_custom_call" | custom-call | flops 679477248 | bytes 18874368 | tf_op jit(solution)/shard_map/pallas_call | solution.py:72
  570.8 19.6 %all-gather.9.cloned.1.call-done.refs_0_ = bf16[2304,256]{1,0:T(8,128)(2,1)} async-done(((bf16[576,256]{1,0:T(8,128)(2,1)}), bf16[2304,256]{1,0:T(8,128)(2,1)}) %all-gather.9.cloned.1.call-update) | async-done | bytes 1179664 | tf_op jit(solution)/shard_map/all_gather | solution.py:193
  590.4 1.9 fusion.1
  592.4 0.7 reshape.123
  593.1 0.8 copy.97
  593.9 3.7 all-to-all-start.3
  598.1 2.6 shard_map.106
  600.8 5.6 all-to-all-done.3
  606.5 1.7 gather_fusion
  608.6 2.0 multiply_reduce_fusion
  (48 shorter events, 2.9 us)
Async XLA Ops:
  7.2 200.4 %all-gather.5.cloned.1.call-start = ((), (), s32[]{:S(2)}) async-start(), calls=%async_computation.4 | async-start | bytes 13271040 | tf_op jit(solution)/shard_map/all_gather | solution.py:159
  18.7 375.3 %all-gather.7.cloned.1.call-start = ((), (), s32[]{:S(2)}) async-start(), calls=%async_computation.5 | async-start | bytes 13271040 | tf_op jit(solution)/shard_map/all_gather | solution.py:164
  64.0 496.5 %all-gather.11.cloned.1.call-start = ((), (), s32[]{:S(2)}) async-start(), calls=%async_computation.7 | async-start | bytes 11796480 | tf_op jit(solution)/shard_map/all_gather | solution.py:169
  223.0 5.4 copy-start.3
  223.0 183.8 %all-to-all-start = ((bf16[8,288,2304]{2,1,0:T(8,128)(2,1)}), bf16[8,288,2304]{2,1,0:T(8,128)(2,1)}, u32[]{:S(2)}, u32[]{:S(2)}) async-start(bf16[8,288,2304]{2,1,0:T(8,128)(2,1)} %bitcast.54), calls=%async_computation | async-start | bytes 21233664 | tf_op jit(solution)/shard_map/all_to_all | solution.py:155
  228.3 362.1 %all-gather.9.cloned.1.call-start = ((), (), s32[]{:S(2)}) async-start(), calls=%async_computation.6 | async-start | bytes 1474560 | tf_op jit(solution)/shard_map/all_gather | solution.py:193
  229.7 3.5 copy-start.1
  406.9 13.6 %copy-start = (bf16[72,2304]{1,0:T(8,128)(2,1)S(1)}, bf16[72,2304]{1,0:T(8,128)(2,1)}, u32[]{:S(2)}) copy-start(bf16[72,2304]{1,0:T(8,128)(2,1)} %convolution_convert_fusion.chosen_ref) | copy-start | bytes 995332
  427.4 1.0 copy-start.2
  429.1 168.9 %copy-start.4 = (f32[192,2]{0,1:T(2,128)S(1)}, f32[192,2]{0,1:T(2,128)}, u32[]{:S(2)}) copy-start(f32[192,2]{0,1:T(2,128)} %param.13) | copy-start | bytes 4612
  593.9 12.5 %all-to-all-start.3 = ((bf16[72,8,288]{2,0,1:T(8,128)(2,1)}), bf16[72,8,288]{2,0,1:T(8,128)(2,1)S(1)}, u32[]{:S(2)}, u32[]{:S(2)}) async-start(bf16[72,8,288]{2,0,1:T(8,128)(2,1)} %copy.97), calls=%async_computation.3 | async-start | bytes 884736 | tf_op jit(solution)/shard_map/all_to_all | solution.py:205
Sparse Core Ops, SparseCore 0:
  18.8 188.7 all-gather.4
  209.7 184.2 all-gather.6
  395.6 164.9 all-gather.10
  562.0 28.4 all-gather.8

commit v2 on v1

--- a/solution.py
+++ b/solution.py
@@ -54,10 +54,73 @@
     )(*operands)
 
 
-def flip_dot(wide, total_rows, hidden):
-    features, rows = wide.shape
-    size = block_of(rows, total_rows) or rows
-    slots = hidden.shape[0]
+def columns(wide, first, count, *others):
+    size = block_of(first, count, *others)
+    if size is None:
+        return lax.slice_in_dim(wide, first, first + count, axis=1), count, 0
+    return wide, size, first // size
+
+
+def flip_product(wide, first, rows, chosen):
+    features = wide.shape[0]
+    wide, size, start = columns(wide, first, rows)
+    slots = chosen.shape[0]
+
+    def kernel(wide_ref, chosen_ref, rows_ref, product_ref):
+        value = wide_ref[...]
+        rows_ref[...] = value.T
+        product_ref[...] = jnp.dot(chosen_ref[...], value, preferred_element_type=jnp.float32)
+
+    return pl.pallas_call(
+        kernel,
+        grid=(rows // size,),
+        in_specs=[
+            pl.BlockSpec((features, size), lambda i: (0, start + i)),
+            pl.BlockSpec((slots, features), lambda i: (0, 0)),
+        ],
+        out_specs=[
+            pl.BlockSpec((size, features), lambda i: (i, 0)),
+            pl.BlockSpec((slots, size), lambda i: (0, i)),
+        ],
+        out_shape=[
+            jax.ShapeDtypeStruct((rows, features), wide.dtype),
+            jax.ShapeDtypeStruct((slots, rows), jnp.float32),
+        ],
+        cost_estimate=pl.CostEstimate(
+            flops=2 * slots * features * rows,
+            bytes_accessed=4 * features * rows,
+            transcendentals=0,
+        ),
+    )(wide, chosen)
+
+
+def spread(train, gain):
+    experts, features, count = train.shape
+    rows = experts * count
+    size = block_of(rows) or rows
+
+    def kernel(train_ref, gain_ref, out_ref):
+        out_ref[...] = (train_ref[...] * gain_ref[...]).astype(jnp.bfloat16).T
+
+    return pl.pallas_call(
+        kernel,
+        grid=(rows // size,),
+        in_specs=[
+            pl.BlockSpec((size, features), lambda i: (i, 0)),
+            pl.BlockSpec((1, features), lambda i: (0, 0)),
+        ],
+        out_specs=pl.BlockSpec((features, size), lambda i: (0, i)),
+        out_shape=jax.ShapeDtypeStruct((features, rows), jnp.bfloat16),
+        cost_estimate=pl.CostEstimate(
+            flops=train.size, bytes_accessed=6 * train.size, transcendentals=0
+        ),
+    )(train.transpose(0, 2, 1).reshape(rows, features), gain[None, :])
+
+
+def flip_dot(wide, first, total_rows, hidden):
+    features = wide.shape[0]
+    slots, rows = hidden.shape
+    wide, size, start = columns(wide, first, rows, total_rows)
 
     def kernel(wide_ref, hidden_ref, rows_ref, total_ref):
         turned = wide_ref[...].T
@@ -73,7 +136,7 @@
         kernel,
         grid=(rows // size,),
         in_specs=[
-            pl.BlockSpec((features, size), lambda i: (0, i)),
+            pl.BlockSpec((features, size), lambda i: (0, start + i)),
             pl.BlockSpec((slots, size), lambda i: (0, i)),
         ],
         out_specs=[
@@ -147,26 +210,23 @@
     experts = gate_train.shape[0]
     slices = tp_count // experts
     gain_column = gain[None, :, None]
-    gate_round = (gate_train * gain_column).astype(jnp.bfloat16)
     up_round = (up_train * gain_column).astype(jnp.bfloat16)
     down_round = down_train.astype(jnp.bfloat16)
 
     def exchange(matrix):
         return lax.all_to_all(matrix, "tp", split_axis=0, concat_axis=1, tiled=True)
 
-    local_features = gate_train.shape[1]
-    gate_local = arrange(gate_round, tp_count).transpose(2, 0, 1).reshape(local_features, -1)
-    gate_all = lax.all_gather(gate_local, "fs", axis=0, tiled=True)
+    gate_all = lax.all_gather(spread(gate_train, gain), "fs", axis=0, tiled=True)
     features = gate_all.shape[0]
 
     up_moved = exchange(arrange(up_round, tp_count))[0].T
     down_moved = exchange(arrange(down_round, tp_count))[0].T
-    up_wide = lax.all_gather(up_moved, "fs", axis=0, tiled=True)
-
     units = down_moved.shape[1]
     size = block_of(units) or units
     main = units - size if units > size else units
-    down_wide = lax.all_gather(down_moved[:, :main], "fs", axis=0, tiled=True)
+    both_wide = lax.all_gather(
+        jnp.concatenate([up_moved, down_moved[:, :main]], axis=1), "fs", axis=0, tiled=True
+    )
 
     tokens_wide = tokens.astype(jnp.float32)
     normed = (
@@ -184,12 +244,11 @@
 
     gate_moved = exchange(gate_all.reshape(features, tp_count, -1).transpose(1, 2, 0))
     gate_new, gate_pre = keep_dot(gate_moved[0], chosen)
-    up_new = flip(up_wide, units, 0)
-    up_pre = jnp.dot(chosen, up_wide, preferred_element_type=jnp.float32)
+    up_new, up_pre = flip_product(both_wide, 0, units, chosen)
     hidden = (jax.nn.silu(gate_pre) * up_pre).astype(jnp.bfloat16)
-    down_new, partial_value = flip_dot(down_wide, units, hidden[:, :main])
+    down_new, partial_value = flip_dot(both_wide, units, units, hidden[:, :main])
     if main < units:
-        rest_moved = after(down_moved[:, main:], up_new, gate_new, hidden)
+        rest_moved = after(down_moved[:, main:], gate_new)
         rest_wide = lax.all_gather(rest_moved, "fs", axis=0, tiled=True)
         partial_value = partial_value + lax.dot_general(
             hidden[:, main:], rest_wide, contract_last, preferred_element_type=jnp.float32

time: 619 us -> 607 us (0.981)
  blocking collectives: 78.9 us -> 0 us
  waiting for transfers between devices: 410 us -> 465 us
  starting transfers between devices: 9.12 us -> 19 us
  Pallas kernels: 39.4 us -> 47.1 us
  matrix products: 9.96 us -> 3.05 us
    all_to_all x1 -> x3, waiting for transfers between devices: 0.01 us -> 169 us  [exchange(): return lax.all_to_all(matrix, 'tp', split_axis=0, concat_axis=1, tiled=True)]
    all_gather x3 -> x2, waiting for transfers between devices: 385 us -> 285 us  [the longest x1 190 us: shards(): lax.all_gather(jnp.concatenate([up_moved, down_moved[:, :main]], axis=1),...]
    all_to_all x2 -> x0, blocking collectives: 78.9 us -> none  [exchange(): return lax.all_to_all(matrix, 'tp', split_axis=0, concat_axis=1, tiled=True)]
    pallas_call x0 -> x2, Pallas kernels: none -> 20.7 us  [the longest x1 13.1 us: flip_product(): pl.pallas_call(kernel, grid=(rows // size,), in_specs=[pl.BlockSpec((feat...]
    all_gather x1, waiting for transfers between devices: 19.6 us -> 5.15 us  [shards(): rest_wide = lax.all_gather(rest_moved, 'fs', axis=0, tiled=True)]
    pallas_call x2 -> x1, Pallas kernels: 15.5 us -> 2.64 us  [flip(): pl.pallas_call(kernel, grid=(rows // size,), in_specs=in_specs, out_specs...]
    all_to_all x1 -> x3, starting transfers between devices: 5.31 us -> 15.2 us  [exchange(): return lax.all_to_all(matrix, 'tp', split_axis=0, concat_axis=1, tiled=True)]
    dot_general x1 -> x0, matrix products: 6.9 us -> none  [shards(): up_pre = jnp.dot(chosen, up_wide, preferred_element_type=jnp.float32)]
  transfers between devices with their start and end apart: 6 -> 7, of which waited for: 5 -> 7; matrix products, arithmetic and copies ran while one was open for 7% -> 8% of each run, Pallas kernels for 6% -> 7%
where the time goes in v2:
time: 607 us; the launch traced here: 604 us
  waiting for transfers between devices  465 us (77%)
  Pallas kernels  47.1 us (8%)
  local copies, waits for them, and re-layouts  37.4 us (6%)
  other arithmetic  19.3 us (3%)
  starting transfers between devices  19 us (3%)
  between operations  13.9 us (2%)
    all_gather x1, waiting for transfers between devices, shards(): lax.all_gather(jnp.concatenate([up_moved, down_moved[:, :main]], axis=1),...  190 us
    all_to_all x3, waiting for transfers between devices, exchange(): return lax.all_to_all(matrix, 'tp', split_axis=0, concat_axis=1, tiled=True)  169 us
    all_gather x1, waiting for transfers between devices, shards(): lax.all_gather(spread(gate_train, gain), 'fs', axis=0, tiled=True)  95.3 us
    all_gather x1, local copies, waits for them, and re-layouts, shards(): lax.all_gather(spread(gate_train, gain), 'fs', axis=0, tiled=True)  15.6 us
    all_to_all x3, starting transfers between devices, exchange(): return lax.all_to_all(matrix, 'tp', split_axis=0, concat_axis=1, tiled=True)  15.2 us
    pallas_call x1, Pallas kernels, keep_dot(): pl.pallas_call(kernel, grid=(rows // size,), in_specs=[pl.BlockSpec((size...  13.4 us
    pallas_call x1, Pallas kernels, flip_product(): pl.pallas_call(kernel, grid=(rows // size,), in_specs=[pl.BlockSpec((feat...  13.1 us
  transfers between devices with their start and end apart: 7, of which 7 were waited for; matrix products, arithmetic and copies ran while one was open for 8% of the time, Pallas kernels for 7%

profile of v2, /device:TPU:0, one launch (start us, length us, event | category | flops | bytes accessed | tf_op | source)
XLA Modules:
  0.0 604.5 jit_solution(15822619317554677456)
XLA Ops:
  7.2 1.3 broadcast_in_dim.37.gain_ref
  8.5 7.6 %shard_map.102 = bf16[576,2304]{1,0:T(8,128)(2,1)} custom-call(f32[2304,576]{1,0:T(8,128)} %bitcast.53, f32[1,576]{1,0:T(1,128)} %broadcast_in_dim.37.gain_ref), custom_call_target="tpu_custom_call" | custom-call | flops 1327104 | bytes 7962624 | tf_op jit(solution)/shard_map/pallas_call | solution.py:105
  16.1 4.6 convert_bitcast_fusion
  20.7 5.3 all-to-all-start.2
  26.0 5.7 fusion.1
  31.7 30.0 %all-to-all-done.2 = bf16[8,288,576]{2,1,0:T(8,128)(2,1)S(1)} async-done(((bf16[8,288,576]{2,1,0:T(8,128)(2,1)}), bf16[8,288,576]{2,1,0:T(8,128)(2,1)S(1)}, u32[]{:S(2)}, u32[]{:S(2)}) %all-to-all-start.2) | async-done | bytes 2654240 | tf_op jit(solution)/shard_map/all_to_all | solution.py:217
  61.8 4.4 all-to-all-start.1
  66.2 3.5 copy.72
  69.7 3.4 slice.45
  73.1 28.8 %all-to-all-done.1 = bf16[8,288,576]{2,1,0:T(8,128)(2,1)} async-done(((bf16[8,288,576]{2,1,0:T(8,128)(2,1)}), bf16[8,288,576]{2,1,0:T(8,128)(2,1)}, u32[]{:S(2)}, u32[]{:S(2)}) %all-to-all-start.1) | async-done | bytes 2654240 | tf_op jit(solution)/shard_map/all_to_all | solution.py:217
  101.9 3.4 copy.71
  105.4 4.3 pad_maximum_fusion
  109.7 95.3 %all-gather.4.cloned.1.call-done = bf16[2304,2304]{1,0:T(8,128)(2,1)} async-done(((bf16[576,2304]{1,0:T(8,128)(2,1)}), bf16[2304,2304]{1,0:T(8,128)(2,1)}) %all-gather.4.cloned.1.call-update) | async-done | bytes 10616848 | tf_op jit(solution)/shard_map/all_gather | solution.py:219
  205.0 15.6 %copy.70 = bf16[2304,2304]{0,1:T(8,128)(2,1)} copy(bf16[2304,2304]{1,0:T(8,128)(2,1)} %all-gather.4.cloned.1.call-done) | data formatting | bytes 21233664 | tf_op jit(solution)/shard_map/all_gather | solution.py:219
  220.6 5.4 all-to-all-start
  227.4 2.7 gather_fusion.1
  231.2 1.1 convolution_convert_fusion.chosen_ref
  232.3 1.7 slice.46.refs_0_
  234.0 110.0 %all-to-all-done = bf16[8,288,2304]{2,1,0:T(8,128)(2,1)} async-done(((bf16[8,288,2304]{2,1,0:T(8,128)(2,1)}), bf16[8,288,2304]{2,1,0:T(8,128)(2,1)}, u32[]{:S(2)}, u32[]{:S(2)}) %all-to-all-start) | async-done | bytes 10616864 | tf_op jit(solution)/shard_map/all_to_all | solution.py:217
  344.0 13.4 %shard_map.103 = (bf16[2304,2304]{1,0:T(8,128)(2,1)}, f32[72,2304]{1,0:T(8,128)}) custom-call(bf16[2304,2304]{1,0:T(8,128)(2,1)} %bitcast.4.weights_ref, bf16[72,2304]{1,0:T(8,128)(2,1)} %convolution_convert_fusion.chosen_ref), custom_call_target="tpu_custom_call" | custom-call | flops 764411904 | bytes 21233664 | tf_op jit(solution)/shard_map/pallas_call | solution.py:172
  357.5 189.8 %all-gather.6.cloned.1.call-done.wide_ref = bf16[2304,4352]{1,0:T(8,128)(2,1)} async-done(((bf16[576,4352]{1,0:T(8,128)(2,1)}), bf16[2304,4352]{1,0:T(8,128)(2,1)}) %all-gather.6.cloned.1.call-update) | async-done | bytes 20054032 | tf_op jit(solution)/shard_map/all_gather | solution.py:227
  547.2 13.1 %shard_map.104 = (bf16[2304,2304]{1,0:T(8,128)(2,1)}, f32[72,2304]{1,0:T(8,128)}) custom-call(bf16[2304,4352]{1,0:T(8,128)(2,1)} %all-gather.6.cloned.1.call-done.wide_ref, bf16[72,2304]{1,0:T(8,128)(2,1)} %convolution_convert_fusion.chosen_ref), custom_call_target="tpu_custom_call" | custom-call | flops 764411904 | bytes 21233664 | tf_op jit(solution)/shard_map/pallas_call | solution.py:74
  560.3 1.3 multiply_convert_fusion.1
  562.3 10.3 %shard_map.106 = (bf16[2304,2304]{1,0:T(8,128)(2,1)}, f32[72,2304]{1,0:T(8,128)}) custom-call(bf16[2304,4352]{1,0:T(8,128)(2,1)} %all-gather.6.cloned.1.call-done.wide_ref, bf16[72,2048]{1,0:T(8,128)(2,1)} %slice.47.hidden_ref), custom_call_target="tpu_custom_call" | custom-call | flops 679477248 | bytes 18874368 | tf_op jit(solution)/shard_map/pallas_call | solution.py:135
  572.6 5.2 all-gather.8.cloned.1.call-done.refs_0_
  577.8 1.9 fusion
  580.4 0.8 copy.77
  581.3 3.7 all-to-all-start.3
  585.5 2.6 shard_map.107
  588.1 5.6 all-to-all-done.3
  593.8 1.7 gather_fusion
  595.9 2.0 multiply_reduce_fusion
  (49 shorter events, 4.9 us)
Async XLA Ops:
  7.2 197.9 %all-gather.4.cloned.1.call-start = ((), (), s32[]{:S(2)}) async-start(), calls=%async_computation.4 | async-start | bytes 13271040 | tf_op jit(solution)/shard_map/all_gather | solution.py:219
  20.7 5.3 copy-start.3
  20.7 41.1 %all-to-all-start.2 = ((bf16[8,288,576]{2,1,0:T(8,128)(2,1)}), bf16[8,288,576]{2,1,0:T(8,128)(2,1)S(1)}, u32[]{:S(2)}, u32[]{:S(2)}) async-start(bf16[8,288,576]{2,1,0:T(8,128)(2,1)} %convert_bitcast_fusion), calls=%async_computation.2 | async-start | bytes 5898240 | tf_op jit(solution)/shard_map/all_to_all | solution.py:217
  61.8 40.2 %all-to-all-start.1 = ((bf16[8,288,576]{2,1,0:T(8,128)(2,1)}), bf16[8,288,576]{2,1,0:T(8,128)(2,1)}, u32[]{:S(2)}, u32[]{:S(2)}) async-start(bf16[8,288,576]{2,1,0:T(8,128)(2,1)} %fusion.1), calls=%async_computation.1 | async-start | bytes 5898240 | tf_op jit(solution)/shard_map/all_to_all | solution.py:217
  66.2 481.0 %all-gather.6.cloned.1.call-start = ((), (), s32[]{:S(2)}) async-start(), calls=%async_computation.5 | async-start | bytes 25067520 | tf_op jit(solution)/shard_map/all_gather | solution.py:227
  220.6 5.5 copy-start.2
  220.6 123.4 %all-to-all-start = ((bf16[8,288,2304]{2,1,0:T(8,128)(2,1)}), bf16[8,288,2304]{2,1,0:T(8,128)(2,1)}, u32[]{:S(2)}, u32[]{:S(2)}) async-start(bf16[8,288,2304]{2,1,0:T(8,128)(2,1)} %bitcast.45), calls=%async_computation | async-start | bytes 21233664 | tf_op jit(solution)/shard_map/all_to_all | solution.py:217
  226.1 351.7 %all-gather.8.cloned.1.call-start = ((), (), s32[]{:S(2)}) async-start(), calls=%async_computation.6 | async-start | bytes 1474560 | tf_op jit(solution)/shard_map/all_gather | solution.py:252
  227.4 3.5 copy-start
  357.5 202.8 %copy-start.1 = (f32[72,2304]{1,0:T(8,128)S(1)}, f32[72,2304]{1,0:T(8,128)}, u32[]{:S(2)}) copy-start(f32[72,2304]{1,0:T(8,128)} %get-tuple-element.12) | copy-start | bytes 1990660
  562.3 23.0 %copy-start.4 = (f32[192,2]{0,1:T(2,128)S(1)}, f32[192,2]{0,1:T(2,128)}, u32[]{:S(2)}) copy-start(f32[192,2]{0,1:T(2,128)} %param.13) | copy-start | bytes 4612
  581.3 12.5 %all-to-all-start.3 = ((bf16[72,8,288]{2,0,1:T(8,128)(2,1)}), bf16[72,8,288]{2,0,1:T(8,128)(2,1)S(1)}, u32[]{:S(2)}, u32[]{:S(2)}) async-start(bf16[72,8,288]{2,0,1:T(8,128)(2,1)} %copy.77), calls=%async_computation.3 | async-start | bytes 884736 | tf_op jit(solution)/shard_map/all_to_all | solution.py:264
Sparse Core Ops, SparseCore 0:
  16.2 188.7 all-gather.3
  207.2 340.0 all-gather.5
  548.8 28.9 all-gather.7
